TPU v7x, 32 devices: a whole 2x2x4 slice. The times are simulated.
32 devices in a mesh: grp: 2 (over y), ep: 16 (over z, x, core), tp: 1.
Axes of the slice: x: 2, y: 2, z: 4, core: 2. Of those that a mesh axis runs over, the one named last changes fastest.
Arguments:
- tokens: bfloat16 [2048, 2048], P(('grp', 'ep')), parts along dimension 0, may hold values from -6 to 6
- norm_gain: float32 [2048], replicated, may hold values from 0.1 to 1.9
- routes: int32 [2048, 6], P(('grp', 'ep')), parts along dimension 0, may hold values from 0 to 15, all different within a row; in each aligned block of 64 rows (0 to 63, 64 to 127, ...) at most 48 rows name the same one
- route_weights: float32 [2048, 6], P(('grp', 'ep')), parts along dimension 0, may hold values from 0.05 to 1
- w_gate: bfloat16 [16, 2048, 2048], P('ep', None, 'tp'), may hold values from -0.125 to 0.125
- w_up: bfloat16 [16, 2048, 2048], P('ep', None, 'tp'), may hold values from -0.125 to 0.125
- w_down: bfloat16 [16, 2048, 2048], P('ep', 'tp'), may hold values from -4 to 4
- final_gain: float32 [2048], P('tp'), may hold values from 0.1 to 1.9
Outputs:
- mixed_out: bfloat16 [2048, 2048], P(('grp', 'ep'), 'tp'), parts along dimension 0
There are 2 independent parts, one for each index of `grp`. A program takes and returns all parts, laid end to end along the dimension named above; an argument that names none is the same for every part. Nothing has to cross between parts.
Inputs may be any that keep to these rules, and one draw needn't show every extreme that they name: `routes`: each row names 6 different experts; within the rows of one index of ep no expert is named by more than 48 rows, and in every draw some expert is named by exactly 48 rows of some index.
All inputs are finite; a program needn't handle non-finite values.
Results may differ from a plain program's by a relative error of at most 0.015.
Values may be sent and summed in bfloat16 or wider, within the bound.
No kernel may reach another device: no remote copies, remote signals or barrier semaphores. Data moves between devices by JAX's collectives and lax.ppermute only.
A program may use at most 64 MiB of HBM per device.

v0:
```python
import jax
import jax.numpy as jnp
from jax import lax
from jax.sharding import PartitionSpec as P

TOP_K = 6


EPS = 1e-06


def slot_table(route_rows, experts_all, capacity):
    flattened = route_rows.reshape(-1)
    matches = (flattened[:, None] == jnp.arange(experts_all, dtype=jnp.int32)[None, :]).astype(
        jnp.int32
    )
    earlier = jnp.cumsum(matches, axis=0) - matches
    slot_of = jnp.sum(earlier * matches, axis=1)
    return (flattened * capacity + slot_of).reshape(route_rows.shape)


def per_device(tokens, norm_gain, routes, route_weights, w_gate, w_up, w_down, final_gain):
    tok_count, features = tokens.shape
    ep_size = lax.axis_size("ep")
    exp_local = w_gate.shape[0]
    experts_all = exp_local * ep_size
    capacity = max(2, min(tok_count, 2 * tok_count * TOP_K // experts_all))
    slot_count = experts_all * capacity
    tokens_f = tokens.astype(jnp.float32)
    inverse = lax.rsqrt(jnp.mean(tokens_f * tokens_f, axis=1, keepdims=True) + EPS)
    normed = (tokens_f * inverse * norm_gain[None, :]).astype(jnp.bfloat16)
    places = slot_table(routes, experts_all, capacity)
    slot_ids = jnp.arange(slot_count, dtype=jnp.int32)
    matched = places[:, :, None] == slot_ids[None, None, :]
    selector = jnp.sum(matched.astype(jnp.float32), axis=1).T.astype(jnp.bfloat16)
    combine_rows = jnp.sum(jnp.where(matched, route_weights[:, :, None], 0.0), axis=1)
    outgoing = jnp.dot(selector, normed, preferred_element_type=jnp.float32).astype(jnp.bfloat16)
    outgoing = outgoing.reshape(ep_size, exp_local, capacity, features)
    received = lax.all_to_all(outgoing, "ep", split_axis=0, concat_axis=0, tiled=True)
    gate_value = jnp.einsum("secd,edf->secf", received, w_gate, preferred_element_type=jnp.float32)
    up_value = jnp.einsum("secd,edf->secf", received, w_up, preferred_element_type=jnp.float32)
    hidden = (jax.nn.silu(gate_value) * up_value).astype(jnp.bfloat16)
    partial_value = jnp.einsum("secf,efd->secd", hidden, w_down, preferred_element_type=jnp.float32)
    summed = lax.psum_scatter(
        partial_value.astype(jnp.bfloat16), "tp", scatter_dimension=3, tiled=True
    )
    returned = lax.all_to_all(summed, "ep", split_axis=0, concat_axis=0, tiled=True)
    results = returned.reshape(slot_count, returned.shape[3]).astype(jnp.float32)
    combined = jnp.dot(combine_rows, results, precision=lax.Precision.HIGHEST)
    local_squares = jnp.sum(combined * combined, axis=1)
    squares_all = lax.psum(local_squares, "tp")
    inverse_out = lax.rsqrt(squares_all / features + EPS)
    return (combined * inverse_out[:, None] * final_gain[None, :]).astype(jnp.bfloat16)


def solution(mesh):
    placed = (
        P(("grp", "ep"), None),
        P(),
        P(("grp", "ep"), None),
        P(("grp", "ep"), None),
        P("ep", None, "tp"),
        P("ep", None, "tp"),
        P("ep", "tp", None),
        P("tp"),
    )
    return jax.shard_map(
        per_device, mesh=mesh, in_specs=placed, out_specs=P(("grp", "ep"), "tp"), check_vma=False
    )
```

profile of v0, /device:TPU:1, one launch (start us, length us, event | category | flops | bytes accessed | tf_op | source)
XLA Modules:
  0.0 194.4 jit_solution(3700836418852448338)
XLA Ops:
  0.0 0.8 copy.33
  0.8 0.1 eq.42
  0.9 0.1 eq.38
  1.1 1.1 fusion.33
  2.2 0.9 reduce-window.6
  3.1 0.2 slice_reduce_fusion
  3.3 0.1 fusion.42
  3.4 0.1 reduce_sum.48
  3.6 0.1 copy.36
  3.6 0.0 copy-start.1
  3.6 0.9 multiply_add_fusion
  4.5 1.1 convert_reduce_fusion
  5.6 2.4 %convolution_convert_fusion = bf16[768,2048]{1,0:T(8,128)(2,1)S(1)} fusion(bf16[64,2048]{1,0:T(8,128)(2,1)} %param.8, f32[2048]{0:T(1024)} %param.9, f32[64]{0:T(128)S(1)} %add_rsqrt_fusion.1, bf16[64,768]{1,0:T(8,128)(2,1)S(1)} %get-tuple-element.5), kind=kOutput, calls=%fused_computation.14 | convolution fusion | flops 203423744 | bytes 3514624 | tf_op jit(solution)/shard_map/dot_general | solution.py:37
  8.0 77.3 %all_to_all.10 = bf16[16,1,48,2048]{3,2,1,0:T(8,128)(2,1)S(1)} all-to-all(bf16[16,1,48,2048]{3,2,1,0:T(8,128)(2,1)S(1)} %bitcast.110), channel_id=1, replica_groups=mesh['grp'=2,'ep'=16,'tp'=1] {'ep'}, dimensions={0} | all-to-all | bytes 6291456 | tf_op jit(solution)/shard_map/all_to_all | solution.py:39
  85.3 0.0 copy-done.1
  85.3 8.6 %fusion.4 = f32[16,48,2048]{2,1,0:T(8,128)} fusion(bf16[1,2048,2048]{2,1,0:T(8,128)(2,1)S(1)} %copy-done.1, bf16[16,1,48,2048]{3,2,1,0:T(8,128)(2,1)S(1)} %all_to_all.10), kind=kOutput, calls=%fused_computation.4 | convolution fusion | flops 6442450944 | bytes 17825792 | tf_op jit(solution)/shard_map/secd,edf->secf/dot_general | solution.py:40
  93.8 22.9 %fusion.24 = bf16[16,1,48,2048]{3,2,1,0:T(8,128)(2,1)} fusion(bf16[1,2048,2048]{2,1,0:T(8,128)(2,1)} %param.14, bf16[1,2048,2048]{2,1,0:T(8,128)(2,1)} %param.13, f32[16,48,2048]{2,1,0:T(8,128)} %fusion.4, bf16[16,1,48,2048]{3,2,1,0:T(8,128)(2,1)S(1)} %all_to_all.10), kind=kOutput, calls=%fused_computation.19 | convolution fusion | flops 12895911936 | bytes 29360128 | tf_op jit(solution)/shard_map/secf,efd->secd/dot_general | solution.py:43
  116.7 0.0 copy-start
  116.7 75.0 %all_to_all.11 = bf16[16,1,48,2048]{3,2,1,0:T(8,128)(2,1)S(1)} all-to-all(bf16[16,1,48,2048]{3,2,1,0:T(8,128)(2,1)} %fusion.24), channel_id=1, replica_groups=mesh['grp'=2,'ep'=16,'tp'=1] {'ep'}, dimensions={0} | all-to-all | bytes 6291456 | tf_op jit(solution)/shard_map/all_to_all | solution.py:47
  191.7 1.9 multiply_reduce_fusion
  193.6 0.0 copy-done
  193.6 0.8 multiply_convert_fusion
  (4 shorter events, 0.1 us)
Async XLA Ops:
  3.6 81.7 %copy-start.1 = (bf16[1,2048,2048]{2,1,0:T(8,128)(2,1)S(1)}, bf16[1,2048,2048]{2,1,0:T(8,128)(2,1)}, u32[]{:S(2)}) copy-start(bf16[1,2048,2048]{2,1,0:T(8,128)(2,1)} %param.12) | copy-start | bytes 25165828
  116.7 76.9 %copy-start = (f32[2048]{0:T(1024)S(1)}, f32[2048]{0:T(1024)}, u32[]{:S(2)}) copy-start(f32[2048]{0:T(1024)} %param.15) | copy-start | bytes 24580
where the time goes:
time: 195 us; the launch traced here: 194 us
  blocking collectives  152 us (78%)
  matrix products  35.7 us (18%)
  other arithmetic  4.93 us (3%)
    all_to_all x1, blocking collectives, per_device(): lax.all_to_all(outgoing, 'ep', split_axis=0, concat_axis=0, tiled=True)  77.3 us
    all_to_all x1, blocking collectives, per_device(): lax.all_to_all(summed, 'ep', split_axis=0, concat_axis=0, tiled=True)  75 us
    dot_general x1, matrix products, per_device(): jnp.einsum('secf,efd->secd', hidden, w_down, preferred_element_type=jnp.f...  22.9 us
    dot_general x1, matrix products, per_device(): jnp.einsum('secd,edf->secf', received, w_gate, preferred_element_type=jnp...  8.55 us

commit v1 on v0

v1 whole, which is shorter than its diff:
```python
import jax
import jax.numpy as jnp
from jax import lax
from jax.sharding import PartitionSpec as P

TOP_K = 6
EPS = 1e-06
LANES = 128


def per_device(tokens, norm_gain, routes, route_weights, w_gate, w_up, w_down, final_gain):
    tok_count, features = tokens.shape
    ep_size = lax.axis_size("ep")
    exp_local = w_gate.shape[0]
    experts_all = exp_local * ep_size
    capacity = max(2, min(tok_count, 2 * tok_count * TOP_K // experts_all))
    tokens_f = tokens.astype(jnp.float32)
    inverse = lax.rsqrt(jnp.mean(tokens_f * tokens_f, axis=1, keepdims=True) + EPS)
    normed = (tokens_f * inverse * norm_gain[None, :]).astype(jnp.bfloat16)
    chosen = routes[:, :, None] == jnp.arange(experts_all, dtype=jnp.int32)[None, None, :]
    table = jnp.sum(jnp.where(chosen, route_weights[:, :, None], 0.0), axis=1)
    high = lax.reduce_precision(table, 8, 7)
    low = table - high
    side = jnp.concatenate([high, low], axis=1).astype(jnp.bfloat16)
    pad = -side.shape[1] % LANES
    side = jnp.pad(side, ((0, 0), (0, pad)))
    gathered = lax.all_gather(
        jnp.concatenate([normed, side], axis=1), "ep", axis=0, tiled=False
    )
    rows_all = gathered[:, :, :features]
    side_all = gathered[:, :, features:]
    base = lax.axis_index("ep") * exp_local
    total = jnp.zeros((ep_size, tok_count, features), jnp.float32)
    for e in range(exp_local):
        lanes = jnp.arange(side_all.shape[2], dtype=jnp.int32)
        mine = (lanes == base + e) | (lanes == experts_all + base + e)
        weight = jnp.sum(jnp.where(mine, side_all.astype(jnp.float32), 0.0), axis=2)
        used = weight > 0
        used_f = used.astype(jnp.float32)
        before = jnp.arange(tok_count)[:, None] < jnp.arange(tok_count)[None, :]
        place = jnp.dot(used_f, before.astype(jnp.float32))
        place = jnp.where(used, place.astype(jnp.int32), -1)
        slots = jnp.arange(capacity, dtype=jnp.int32)
        select = (place[:, None, :] == slots[None, :, None]).astype(jnp.bfloat16)
        slot_weight = jnp.sum(select.astype(jnp.float32) * weight[:, None, :], axis=2)
        rows = jnp.einsum("bst,btd->bsd", select, rows_all, preferred_element_type=jnp.float32)
        rows = rows.astype(jnp.bfloat16).reshape(ep_size * capacity, features)
        gate_value = jnp.dot(rows, w_gate[e], preferred_element_type=jnp.float32)
        up_value = jnp.dot(rows, w_up[e], preferred_element_type=jnp.float32)
        hidden = (jax.nn.silu(gate_value) * up_value).astype(jnp.bfloat16)
        value = jnp.dot(hidden, w_down[e], preferred_element_type=jnp.float32)
        value = value * slot_weight.reshape(-1, 1)
        value = value.astype(jnp.bfloat16).reshape(ep_size, capacity, features)
        total = total + jnp.einsum("bst,bsd->btd", select, value, preferred_element_type=jnp.float32)
    total = total.astype(jnp.bfloat16).reshape(ep_size * tok_count, features)
    total = lax.psum_scatter(total, "tp", scatter_dimension=1, tiled=True)
    combined = lax.psum_scatter(total, "ep", scatter_dimension=0, tiled=True).astype(jnp.float32)
    squares_all = lax.psum(jnp.sum(combined * combined, axis=1), "tp")
    inverse_out = lax.rsqrt(squares_all / features + EPS)
    return (combined * inverse_out[:, None] * final_gain[None, :]).astype(jnp.bfloat16)


def solution(mesh):
    placed = (
        P(("grp", "ep"), None),
        P(),
        P(("grp", "ep"), None),
        P(("grp", "ep"), None),
        P("ep", None, "tp"),
        P("ep", None, "tp"),
        P("ep", "tp", None),
        P("tp"),
    )
    return jax.shard_map(
        per_device, mesh=mesh, in_specs=placed, out_specs=P(("grp", "ep"), "tp"), check_vma=False
    )
```

time: 195 us -> 190 us (0.974); the launches traced: 194 us -> 187 us
  blocking collectives: 152 us -> 0 us
  waiting for transfers between devices: 0 us -> 124 us
  between operations: 0.06 us -> 13.5 us
  matrix products: 35.7 us -> 41.9 us
  other arithmetic: 4.93 us -> 7.9 us
    all_to_all x2 -> x0, blocking collectives: 152 us -> none  [the longest x1 77.3 us: per_device(): lax.all_to_all(outgoing, 'ep', split_axis=0, concat_axis=0, tiled=True)]
    reduce_scatter x0 -> x1, waiting for transfers between devices: none -> 69.6 us  [per_device(): lax.psum_scatter(total, 'ep', scatter_dimension=0, tiled=True)]
    all_gather x0 -> x1, waiting for transfers between devices: none -> 54.2 us  [per_device(): lax.all_gather(jnp.concatenate([normed, side], axis=1), 'ep', axis=0, til...]
    dot_general x4 -> x5, matrix products: 35.7 us -> 41.9 us  [the longest x1 22.9 us: per_device(): value = jnp.dot(hidden, w_down[e], preferred_element_type=jnp.float32)]
    reduce_sum x2 -> x4, other arithmetic: 1.21 us -> 3.17 us  [the longest x1 1.16 us: per_device(): weight = jnp.sum(jnp.where(mine, side_all.astype(jnp.float32), 0.0), axis=2)]
  transfers between devices with their start and end apart: 0 -> 2, of which waited for: 0 -> 2; matrix products, arithmetic and copies ran while one was open for 0% -> 0% of each run, Pallas kernels for 0% -> 0%
where the time goes in v1:
time: 190 us; the launch traced here: 187 us
  waiting for transfers between devices  124 us (65%)
  matrix products  41.9 us (22%)
  between operations  13.5 us (7%)
  other arithmetic  7.9 us (4%)
    reduce_scatter x1, waiting for transfers between devices, per_device(): lax.psum_scatter(total, 'ep', scatter_dimension=0, tiled=True)  69.6 us
    all_gather x1, waiting for transfers between devices, per_device(): lax.all_gather(jnp.concatenate([normed, side], axis=1), 'ep', axis=0, til...  54.2 us
    dot_general x1, matrix products, per_device(): value = jnp.dot(hidden, w_down[e], preferred_element_type=jnp.float32)  22.9 us
    dot_general x1, matrix products, per_device(): gate_value = jnp.dot(rows, w_gate[e], preferred_element_type=jnp.float32)  10.7 us
    dot_general x1, matrix products, per_device(): jnp.einsum('bst,bsd->btd', select, value, preferred_element_type=jnp.floa...  5.13 us
  transfers between devices with their start and end apart: 2, of which 2 were waited for; matrix products, arithmetic and copies ran while one was open for 0% of the time, Pallas kernels for 0%

profile of v1, /device:TPU:1, one launch (start us, length us, event | category | flops | bytes accessed | tf_op | source)
XLA Modules:
  0.0 187.4 jit_solution(17535973025197281260)
XLA Ops:
  6.5 0.0 all-gather.3.cloned.1.call-start
  6.5 1.1 fusion.19
  7.7 0.7 select_reduce_fusion.1
  8.4 0.1 copy.12
  8.5 1.1 fusion.21
  9.6 0.7 fusion.26
  10.3 0.0 all-gather.3.cloned.1.call-update
  10.4 0.0 reduce-scatter.2.cloned.1.call-start
  10.4 54.2 %all-gather.3.cloned.1.call-done = bf16[1024,2176]{1,0:T(8,128)(2,1)} async-done(((bf16[64,2176]{1,0:T(8,128)(2,1)}), bf16[1024,2176]{1,0:T(8,128)(2,1)}) %all-gather.3.cloned.1.call-update) | async-done | bytes 4456464 | tf_op jit(solution)/shard_map/all_gather | solution.py:27
  64.7 1.2 select_reduce_fusion
  65.8 0.1 fusion.17
  66.0 3.2 %fusion.12 = bf16[16,48,2048]{2,1,0:T(8,128)(2,1)S(1)} fusion(bf16[16,64,2176]{2,1,0:T(8,128)(2,1)} %bitcast.24, s32[16,64]{1,0:T(8,128)S(1)} %fusion.17), kind=kOutput, calls=%fused_computation.11 | convolution fusion | flops 202948608 | bytes 7344128 | tf_op jit(solution)/shard_map/bst,btd->bsd/dot_general | solution.py:46
  69.1 0.2 multiply_reduce_fusion
  69.3 0.1 mul.72
  69.4 10.7 %fusion.4 = f32[768,2048]{1,0:T(8,128)} fusion(bf16[768,2048]{1,0:T(8,128)(2,1)S(1)} %bitcast.25, bf16[1,2048,2048]{2,1,0:T(8,128)(2,1)} %param.12), kind=kOutput, calls=%fused_computation.4 | convolution fusion | flops 6442450944 | bytes 17825792 | tf_op jit(solution)/shard_map/dot_general | solution.py:48
  80.0 22.9 %multiply_convert_fusion = bf16[768,2048]{1,0:T(8,128)(2,1)} fusion(bf16[1,2048,2048]{2,1,0:T(8,128)(2,1)} %param.14, f32[768]{0:T(1024)S(1)} %mul.72, f32[768,2048]{1,0:T(8,128)} %fusion.4, bf16[768,2048]{1,0:T(8,128)(2,1)S(1)} %bitcast.26, bf16[1,2048,2048]{2,1,0:T(8,128)(2,1)} %param.13), kind=kOutput, calls=%fused_computation.6 | convolution fusion | flops 12897484800 | bytes 29363200 | tf_op jit(solution)/shard_map/dot_general | solution.py:51
  102.9 0.0 copy-start
  102.9 5.1 %convolution_convert_fusion = bf16[16,64,2048]{2,1,0:T(8,128)(2,1)} fusion(bf16[16,48,2048]{2,1,0:T(8,128)(2,1)} %bitcast.27, s32[16,64]{1,0:T(8,128)S(1)} %fusion.17), kind=kOutput, calls=%fused_computation.10 | convolution fusion | flops 203472896 | bytes 7344128 | tf_op jit(solution)/shard_map/bst,bsd->btd/dot_general | solution.py:54
  108.0 0.0 reduce-scatter.2.cloned.1.call-update
  108.1 69.6 %reduce-scatter.2.cloned.1.call-done = bf16[64,2048]{1,0:T(8,128)(2,1)} async-done(((bf16[1024,2048]{1,0:T(8,128)(2,1)}), bf16[64,2048]{1,0:T(8,128)(2,1)}) %reduce-scatter.2.cloned.1.call-update) | async-done | bytes 262160 | tf_op jit(solution)/shard_map/reduce_scatter | solution.py:57
  177.6 1.1 fusion.22
  178.7 0.0 copy-done
  178.7 1.8 fusion.24
  (5 shorter events, 0.0 us)
Async XLA Ops:
  6.5 58.1 %all-gather.3.cloned.1.call-start = ((), (), s32[]{:S(2)}) async-start(), calls=%async_computation.2 | async-start | bytes 4734976 | tf_op jit(solution)/shard_map/all_gather | solution.py:27
  10.4 167.3 %reduce-scatter.2.cloned.1.call-start = ((), (), s32[]{:S(2)}) async-start(), calls=%async_computation.1 | async-start | bytes 4456448 | tf_op jit(solution)/shard_map/reduce_scatter | solution.py:57
  102.9 75.8 %copy-start = (f32[2048]{0:T(1024)S(1)}, f32[2048]{0:T(1024)}, u32[]{:S(2)}) copy-start(f32[2048]{0:T(1024)} %param.15) | copy-start | bytes 24580
Sparse Core Ops, SparseCore 0:
  10.5 54.1 all-gather.2
  108.2 69.3 reduce-scatter.1
